TPU v7x, 32 devices: a whole 2x2x4 slice. The times are simulated.
32 devices in a mesh: sp: 8 (over z, x), tp: 4 (over y, core).
Axes of the slice: x: 2, y: 2, z: 4, core: 2. Of those that a mesh axis runs over, the one named last changes fastest.
Arguments:
- resid: bfloat16 [1024, 2048], P('sp'), may hold values from -8 to 8
- a_val: bfloat16 [1024, 1024], P('sp', 'tp'), may hold values from -8 to 8
- a_gate: bfloat16 [1024, 1024], P('sp', 'tp'), may hold values from -6 to 6
- conv_kernel: bfloat16 [31, 1024], P(None, 'tp'), may hold values from -1 to 1
- conv_bias: float32 [1024], P('tp'), may hold values from -3 to 3
- ln_gain: float32 [1024], P('tp'), may hold values from 0.1 to 1.9
- ln_bias: float32 [1024], P('tp'), may hold values from -3 to 3
- w_out: bfloat16 [1024, 2048], P('tp'), may hold values from -0.1875 to 0.1875
- ffn_gain: float32 [2048], replicated, may hold values from 0.1 to 1.9
- routes: int32 [1024, 4], P('sp'), may hold values from 0 to 7, all different within a row; in each aligned block of 128 rows (0 to 127, 128 to 255, ...) at most 128 rows name the same one
- route_weights: float32 [1024, 4], P('sp'), may hold values from 0.15 to 1.2
- exp_gate: bfloat16 [8, 2048, 4096], P('sp', None, 'tp'), may hold values from -0.125 to 0.125
- exp_up: bfloat16 [8, 2048, 4096], P('sp', None, 'tp'), may hold values from -0.125 to 0.125
- exp_down: bfloat16 [8, 4096, 2048], P('sp', None, 'tp'), may hold values from -0.09375 to 0.09375
- sh_gate: bfloat16 [2048, 512], P(None, 'tp'), may hold values from -0.125 to 0.125
- sh_up: bfloat16 [2048, 512], P(None, 'tp'), may hold values from -0.125 to 0.125
- sh_down: bfloat16 [512, 2048], P(None, 'tp'), may hold values from -0.25 to 0.25
Outputs:
- result: bfloat16 [1024, 2048], P('sp', 'tp')
Inputs may be any that keep to these rules, and one draw needn't show every extreme that they name: `routes`: among the 128 rows of one index of sp, each expert is named at most 128 times, a bound that some block reaches; a row names 4 different experts.
All inputs are finite; a program needn't handle non-finite values.
Results may differ from a plain program's by a relative error of at most 0.007.
Values may be sent and summed in bfloat16 or wider, within the bound.
A program may use at most 64 MiB of HBM per device.

v0:
```python
import jax
import jax.numpy as jnp
from jax import lax
from jax.sharding import PartitionSpec as P

LN_EPS = 1e-05
RMS_EPS = 1e-06


def shifted(value, axis, by):
    size = lax.axis_size(axis)
    pairs = [(i, i + by) for i in range(size) if 0 <= i + by < size]
    return lax.ppermute(value, axis, pairs)


def body(
    resid,
    a_val,
    a_gate,
    conv_kernel,
    conv_bias,
    ln_gain,
    ln_bias,
    w_out,
    ffn_gain,
    routes,
    route_weights,
    exp_gate,
    exp_up,
    exp_down,
    sh_gate,
    sh_up,
    sh_down,
):
    tp_count = lax.axis_size("tp")
    tp_place = lax.axis_index("tp")
    sp_count = lax.axis_size("sp")
    tok_rows = resid.shape[0]
    model_width = resid.shape[1]
    col_width = model_width // tp_count
    col_start = tp_place * col_width
    conv_span = conv_kernel.shape[0]
    channels_all = a_val.shape[1] * tp_count
    gated_in = (a_val.astype(jnp.float32) * jax.nn.sigmoid(a_gate.astype(jnp.float32))).astype(
        jnp.bfloat16
    )
    before = shifted(gated_in[tok_rows - (conv_span - 1) :], "sp", 1)
    padded = jnp.concatenate([before, gated_in], axis=0).astype(jnp.float32)
    kernel = conv_kernel.astype(jnp.float32)

    def add_tap(offset, running):
        window_rows = lax.dynamic_slice_in_dim(padded, offset, tok_rows, 0)
        return running + lax.dynamic_slice_in_dim(kernel, offset, 1, 0) * window_rows

    start_sum = jnp.broadcast_to(conv_bias[None, :], gated_in.shape)
    conv_out = lax.fori_loop(0, conv_span, add_tap, start_sum)
    row_sums = lax.psum((jnp.sum(conv_out, axis=1), jnp.sum(conv_out * conv_out, axis=1)), "tp")
    channel_mean = row_sums[0] / channels_all
    channel_var = row_sums[1] / channels_all - channel_mean * channel_mean
    scaled = (conv_out - channel_mean[:, None]) * lax.rsqrt(
        channel_var[:, None] + LN_EPS
    ) * ln_gain[None, :] + ln_bias[None, :]
    mixed_out = jax.nn.silu(scaled).astype(jnp.bfloat16)
    partial_proj = jnp.dot(mixed_out, w_out, preferred_element_type=jnp.float32)
    projected = lax.psum(partial_proj, "tp")
    middle = (resid.astype(jnp.float32) + projected).astype(jnp.bfloat16)
    middle_f = middle.astype(jnp.float32)
    inverse = lax.rsqrt(jnp.mean(middle_f * middle_f, axis=1, keepdims=True) + RMS_EPS)
    normed = (middle_f * inverse * ffn_gain[None, :]).astype(jnp.bfloat16)
    middle_cols = lax.dynamic_slice_in_dim(middle, col_start, col_width, 1)
    shared_gate = jnp.dot(normed, sh_gate, preferred_element_type=jnp.float32)
    shared_up = jnp.dot(normed, sh_up, preferred_element_type=jnp.float32)
    shared_hidden = (jax.nn.silu(shared_gate) * shared_up).astype(jnp.bfloat16)
    weight_rows = sh_down
    shared = jnp.dot(
        lax.all_gather(shared_hidden, "tp", axis=1, tiled=True),
        weight_rows,
        preferred_element_type=jnp.float32,
    )
    top_count = routes.shape[1]
    local_experts = exp_gate.shape[0]
    experts_all = local_experts * sp_count
    capacity = max(2 * tok_rows * top_count // experts_all, tp_count)
    pair_count = tok_rows * top_count
    chosen = routes.reshape(pair_count)
    one_hot = (chosen[:, None] == jnp.arange(experts_all, dtype=jnp.int32)[None, :]).astype(
        jnp.int32
    )
    earlier = jnp.cumsum(one_hot, axis=0) - one_hot
    place_in = jnp.sum(earlier * one_hot, axis=1)
    slot_of = chosen * capacity + place_in
    owner_ids = (
        jnp.zeros((experts_all * capacity,), jnp.int32)
        .at[slot_of]
        .set(jnp.arange(pair_count, dtype=jnp.int32) + 1)
    )
    owner_grid = owner_ids.reshape(sp_count, local_experts, capacity)
    part_slots = capacity // tp_count
    own_owners = lax.dynamic_slice_in_dim(owner_grid, tp_place * part_slots, part_slots, 2)
    source_row = jnp.maximum(own_owners - 1, 0) // top_count
    taken = normed[source_row.reshape(-1)].reshape(own_owners.shape + (model_width,))
    landed = lax.all_to_all(
        jnp.where((own_owners > 0)[..., None], taken, jnp.zeros((), jnp.bfloat16)),
        "sp",
        split_axis=0,
        concat_axis=0,
        tiled=True,
    )
    arrived = lax.all_gather(landed, "tp", axis=2, tiled=True)
    gate_part = jnp.einsum("sxcd,xdf->sxcf", arrived, exp_gate, preferred_element_type=jnp.float32)
    up_part = jnp.einsum("sxcd,xdf->sxcf", arrived, exp_up, preferred_element_type=jnp.float32)
    expert_hidden = (jax.nn.silu(gate_part) * up_part).astype(jnp.bfloat16)
    weight_rows = exp_down
    expert_sum = jnp.einsum(
        "sxcf,xfd->sxcd",
        lax.all_gather(expert_hidden, "tp", axis=3, tiled=True),
        weight_rows,
        preferred_element_type=jnp.float32,
    )
    expert_out = expert_sum.astype(jnp.bfloat16)
    returned = lax.all_to_all(expert_out, "sp", split_axis=0, concat_axis=0, tiled=True)
    flat_out = returned.reshape(experts_all * capacity, col_width)
    picked = flat_out[slot_of].astype(jnp.float32).reshape(tok_rows, top_count, col_width)
    routed = jnp.sum(picked * route_weights[:, :, None], axis=1)
    return (middle_cols.astype(jnp.float32) + shared + routed).astype(jnp.bfloat16)


def solution(mesh):
    in_specs = (
        P("sp", None),
        P("sp", "tp"),
        P("sp", "tp"),
        P(None, "tp"),
        P("tp"),
        P("tp"),
        P("tp"),
        P("tp", None),
        P(),
        P("sp", None),
        P("sp", None),
        P("sp", None, "tp"),
        P("sp", None, "tp"),
        P("sp", None, "tp"),
        P(None, "tp"),
        P(None, "tp"),
        P(None, "tp"),
    )
    out_specs = P("sp", "tp")
    return jax.shard_map(body, mesh=mesh, in_specs=in_specs, out_specs=out_specs, check_vma=False)
```

profile of v0, /device:TPU:0, one launch (start us, length us, event | category | flops | bytes accessed | tf_op | source)
XLA Modules:
  0.0 262.0 jit_solution(12313480295030517520)
XLA Ops:
  6.5 1.0 multiply_convert_fusion.1
  7.6 4.9 %collective-permute-start = (bf16[30,256]{1,0:T(8,128)(2,1)S(1)}, bf16[30,256]{1,0:T(8,128)(2,1)S(1)}, u32[]{:S(2)}, u32[]{:S(2)}) collective-permute-start(bf16[30,256]{1,0:T(8,128)(2,1)S(1)} %slice.16), channel_id=1, source_target_pairs={{0,4},{4,8},{8,12},{12,16},{16,20},{20,24},{24,28},{1,5},{5,9},{9,... | collective-permute-start | bytes 46088 | tf_op jit(solution)/shard_map/ppermute | solution.py:13
  12.5 0.7 broadcast_multiply_fusion
  13.2 0.8 copy.24
  13.9 0.1 eq.29
  14.1 0.1 eq.25
  14.2 0.0 copy-start.2
  14.2 0.1 copy.23
  14.3 0.1 mul.137
  14.4 1.1 reduce-window.6
  15.6 0.2 slice_reduce_fusion
  15.8 0.1 fusion.40
  15.9 0.7 convert_element_type.69
  16.7 2.4 scatter_custom_fusion
  19.1 0.7 broadcast_in_dim.14
  19.8 2.4 while.13
  22.3 0.1 fusion.46
  22.4 6.3 %all-reduce = (f32[128]{0:T(128)S(1)}, f32[128]{0:T(128)S(1)}) all-reduce(f32[128]{0:T(128)S(1)} %get-tuple-element.86, f32[128]{0:T(128)S(1)} %get-tuple-element.85), channel_id=1, replica_groups=mesh['sp'=8,'tp'=4] {'tp'}, use_global_device_ids=true, to_apply=%region_5.0 | all-reduce | flops 256 | bytes 2048 | tf_op jit(solution)/shard_map/psum | solution.py:57
  28.7 2.1 fusion.33
  30.8 0.0 all-reduce.3.cloned.1.call-update
  30.9 0.0 all-gather.3.cloned.1.call-start
  30.9 0.1 add_select_fusion
  31.0 0.1 reshape.144
  31.1 0.1 compare_bitcast_fusion
  31.2 36.0 %all-reduce.3.cloned.1.call-done = f32[128,2048]{1,0:T(8,128)} async-done(((f32[128,2048]{1,0:T(8,128)}), f32[128,2048]{1,0:T(8,128)}) %all-reduce.3.cloned.1.call-update) | async-done | bytes 1048592 | tf_op jit(solution)/shard_map/psum | solution.py:65
  67.2 1.5 fusion.30
  68.7 0.2 fusion.32
  68.9 1.4 gather_fusion
  70.2 0.1 broadcast_select_fusion
  70.4 30.6 %all_to_all.10 = bf16[8,1,32,2048]{3,2,1,0:T(8,128)(2,1)} all-to-all(bf16[8,1,32,2048]{3,2,1,0:T(8,128)(2,1)S(1)} %broadcast_select_fusion), channel_id=1, replica_groups=mesh['sp'=8,'tp'=4] {'sp'}, dimensions={0} | all-to-all | bytes 2097152 | tf_op jit(solution)/shard_map/all_to_all | solution.py:102
  101.0 0.0 all-gather.3.cloned.1.call-update
  101.1 0.0 all-gather.5.cloned.1.call-start
  101.1 33.4 %all-gather.3.cloned.1.call-done = bf16[8,1,128,2048]{3,2,0,1:T(8,128)(2,1)} async-done(((bf16[8,1,32,2048]{3,2,0,1:T(8,128)(2,1)}), bf16[8,1,128,2048]{3,2,0,1:T(8,128)(2,1)}) %all-gather.3.cloned.1.call-update) | async-done | bytes 4194320 | tf_op jit(solution)/shard_map/all_gather | solution.py:109
  134.6 7.7 %fusion.4 = f32[8,128,1024]{2,1,0:T(8,128)S(1)} fusion(bf16[1,2048,1024]{2,1,0:T(8,128)(2,1)} %param.31, bf16[8,1,128,2048]{3,2,0,1:T(8,128)(2,1)} %all-gather.3.cloned.1.call-done), kind=kOutput, calls=%fused_computation.10 | convolution fusion | flops 4294967296 | bytes 12582912 | tf_op jit(solution)/shard_map/sxcd,xdf->sxcf/dot_general | solution.py:111
  142.2 6.4 %fusion.2 = bf16[8,1,128,1024]{3,2,0,1:T(8,128)(2,1)} fusion(f32[8,128,1024]{2,1,0:T(8,128)S(1)} %fusion.4, bf16[1,2048,1024]{2,1,0:T(8,128)(2,1)S(1)} %copy-done.4, bf16[8,1,128,2048]{3,2,0,1:T(8,128)(2,1)S(1)} %copy-done.5), kind=kOutput, calls=%fused_computation.8 | convolution fusion | flops 4301258752 | bytes 14680064 | tf_op jit(solution)/shard_map/sxcd,xdf->sxcf/dot_general | solution.py:110
  148.6 0.0 all-gather.5.cloned.1.call-update
  148.6 58.4 %all-gather.5.cloned.1.call-done = bf16[8,1,128,4096]{3,2,0,1:T(8,128)(2,1)} async-done(((bf16[8,1,128,1024]{3,2,0,1:T(8,128)(2,1)}), bf16[8,1,128,4096]{3,2,0,1:T(8,128)(2,1)}) %all-gather.5.cloned.1.call-update) | async-done | bytes 8388624 | tf_op jit(solution)/shard_map/all_gather | solution.py:116
  207.0 10.1 %fusion.22 = bf16[8,1,128,512]{3,2,1,0:T(8,128)(2,1)} fusion(bf16[1,4096,512]{2,1,0:T(8,128)(2,1)} %param.32, bf16[8,1,128,4096]{3,2,0,1:T(8,128)(2,1)} %all-gather.5.cloned.1.call-done), kind=kOutput, calls=%fused_computation.22 | convolution fusion | flops 4295491584 | bytes 13631488 | tf_op jit(solution)/shard_map/sxcf,xfd->sxcd/dot_general | solution.py:114
  217.2 5.5 %all-to-all-start.1 = ((bf16[8,1,128,512]{3,2,1,0:T(8,128)(2,1)}), bf16[8,1,128,512]{3,2,1,0:T(8,128)(2,1)S(1)}, u32[]{:S(2)}, u32[]{:S(2)}) async-start(bf16[8,1,128,512]{3,2,1,0:T(8,128)(2,1)} %fusion.22), calls=%async_computation.1 | async-start | bytes 2097152 | tf_op jit(solution)/shard_map/all_to_all | solution.py:121
  222.7 0.1 copy.29
  222.8 1.3 fusion.47
  224.1 1.3 fusion.29
  225.5 5.4 %all_gather.9 = bf16[128,512]{1,0:T(8,128)(2,1)S(1)} all-gather(bf16[128,128]{1,0:T(8,128)(2,1)S(1)} %fusion.29), channel_id=1, replica_groups=mesh['sp'=8,'tp'=4] {'tp'}, dimensions={1}, use_global_device_ids=true | all-gather | bytes 163840 | tf_op jit(solution)/shard_map/all_gather | solution.py:76
  230.9 17.9 %all-to-all-done.1 = bf16[8,1,128,512]{3,2,1,0:T(8,128)(2,1)S(1)} async-done(((bf16[8,1,128,512]{3,2,1,0:T(8,128)(2,1)}), bf16[8,1,128,512]{3,2,1,0:T(8,128)(2,1)S(1)}, u32[]{:S(2)}, u32[]{:S(2)}) %all-to-all-start.1) | async-done | bytes 1048608 | tf_op jit(solution)/shard_map/all_to_all | solution.py:121
  248.9 2.6 gather_fusion.1
  251.5 1.4 reshape.152
  252.8 0.7 multiply_reduce_fusion
  253.6 1.9 fusion.28
  (87 shorter events, 1.7 us)
Async XLA Ops:
  6.5 22.2 %copy-start = (bf16[256,2048]{1,0:T(8,128)(2,1)S(1)}, bf16[256,2048]{1,0:T(8,128)(2,1)}, u32[]{:S(2)}) copy-start(bf16[256,2048]{1,0:T(8,128)(2,1)} %param.26) | copy-start | bytes 3145732
  6.5 60.7 %copy-start.1 = (bf16[128,2048]{1,0:T(8,128)(2,1)S(1)}, bf16[128,2048]{1,0:T(8,128)(2,1)}, u32[]{:S(2)}) copy-start(bf16[128,2048]{1,0:T(8,128)(2,1)} %param.19) | copy-start | bytes 1572868
  6.5 60.6 %all-reduce.3.cloned.1.call-start = ((), (), s32[]{:S(2)}) async-start(), calls=%async_computation.2 | async-start | bytes 2097152 | tf_op jit(solution)/shard_map/psum | solution.py:65
  7.6 11.5 %collective-permute-start = (bf16[30,256]{1,0:T(8,128)(2,1)S(1)}, bf16[30,256]{1,0:T(8,128)(2,1)S(1)}, u32[]{:S(2)}, u32[]{:S(2)}) collective-permute-start(bf16[30,256]{1,0:T(8,128)(2,1)S(1)} %slice.16), channel_id=1, source_target_pairs={{0,4},{4,8},{8,12},{12,16},{16,20},{20,24},{24,28},{1,5},{5,9},{9,... | collective-permute-start | bytes 46088 | tf_op jit(solution)/shard_map/ppermute | solution.py:13
  14.2 54.5 %copy-start.2 = (f32[2048]{0:T(1024)S(1)}, f32[2048]{0:T(1024)}, u32[]{:S(2)}) copy-start(f32[2048]{0:T(1024)} %param.27) | copy-start | bytes 24580
  30.9 103.7 %all-gather.3.cloned.1.call-start = ((), (), s32[]{:S(2)}) async-start(), calls=%async_computation.3 | async-start | bytes 5242880 | tf_op jit(solution)/shard_map/all_gather | solution.py:109
  101.1 106.0 %all-gather.5.cloned.1.call-start = ((), (), s32[]{:S(2)}) async-start(), calls=%async_computation.4 | async-start | bytes 10485760 | tf_op jit(solution)/shard_map/all_gather | solution.py:116
  134.5 7.7 %copy-start.4 = (bf16[1,2048,1024]{2,1,0:T(8,128)(2,1)S(1)}, bf16[1,2048,1024]{2,1,0:T(8,128)(2,1)}, u32[]{:S(2)}) copy-start(bf16[1,2048,1024]{2,1,0:T(8,128)(2,1)} %param.30) | copy-start | bytes 12582916
  134.5 7.7 %copy-start.5 = (bf16[8,1,128,2048]{3,2,0,1:T(8,128)(2,1)S(1)}, bf16[8,1,128,2048]{3,2,0,1:T(8,128)(2,1)}, u32[]{:S(2)}) copy-start(bf16[8,1,128,2048]{3,2,0,1:T(8,128)(2,1)} %all-gather.3.cloned.1.call-done) | copy-start | bytes 12582916
  148.6 74.0 %copy-start.3 = (f32[128,4]{0,1:T(4,128)S(1)}, f32[128,4]{0,1:T(4,128)}, u32[]{:S(2)}) copy-start(f32[128,4]{0,1:T(4,128)} %param.29) | copy-start | bytes 6148
  217.2 31.7 %all-to-all-start.1 = ((bf16[8,1,128,512]{3,2,1,0:T(8,128)(2,1)}), bf16[8,1,128,512]{3,2,1,0:T(8,128)(2,1)S(1)}, u32[]{:S(2)}, u32[]{:S(2)}) async-start(bf16[8,1,128,512]{3,2,1,0:T(8,128)(2,1)} %fusion.22), calls=%async_computation.1 | async-start | bytes 2097152 | tf_op jit(solution)/shard_map/all_to_all | solution.py:121
Sparse Core Ops, SparseCore 0:
  31.0 36.1 all-reduce.2
  101.2 33.3 all-gather.2
  148.7 58.2 all-gather.4
where the time goes:
time: 263 us; the launch traced here: 262 us
  waiting for transfers between devices  146 us (56%)
  blocking collectives  42.4 us (16%)
  matrix products  30.9 us (12%)
  between operations  13.3 us (5%)
  starting transfers between devices  10.5 us (4%)
  local copies, waits for them, and re-layouts  10.4 us (4%)
  other arithmetic  7.78 us (3%)
    all_gather x1, waiting for transfers between devices, body(): lax.all_gather(expert_hidden, 'tp', axis=3, tiled=True)  58.4 us
    psum x1, waiting for transfers between devices, body(): projected = lax.psum(partial_proj, 'tp')  36 us
    all_gather x1, waiting for transfers between devices, body(): arrived = lax.all_gather(landed, 'tp', axis=2, tiled=True)  33.4 us
    all_to_all x1, blocking collectives, body(): lax.all_to_all(jnp.where((own_owners > 0)[..., None], taken, jnp.zeros(()...  30.6 us
    all_to_all x1, waiting for transfers between devices, body(): lax.all_to_all(expert_out, 'sp', split_axis=0, concat_axis=0, tiled=True)  17.9 us
    dot_general x1, matrix products, body(): jnp.einsum('sxcf,xfd->sxcd', lax.all_gather(expert_hidden, 'tp', axis=3,...  10.1 us
    dot_general x1, matrix products, body(): jnp.einsum('sxcd,xdf->sxcf', arrived, exp_up, preferred_element_type=jnp....  7.65 us
    dot_general x1, matrix products, body(): jnp.einsum('sxcd,xdf->sxcf', arrived, exp_gate, preferred_element_type=jn...  6.37 us
  transfers between devices with their start and end apart: 5, of which 4 were waited for; matrix products, arithmetic and copies ran while one was open for 4% of the time, Pallas kernels for 0%

commit v1 on v0

--- a/solution.py
+++ b/solution.py
@@ -113,7 +113,7 @@
     weight_rows = exp_down
     expert_sum = jnp.einsum(
         "sxcf,xfd->sxcd",
-        lax.all_gather(expert_hidden, "tp", axis=3, tiled=True),
+        jnp.concatenate(lax.all_gather(expert_hidden, "tp"), axis=3),
         weight_rows,
         preferred_element_type=jnp.float32,
     )

time: 263 us -> 290 us (1.10)
  local copies, waits for them, and re-layouts: 10.4 us -> 36.9 us
    another operation x1 -> x2, local copies, waits for them, and re-layouts: 0.01 us -> 14.4 us
    all_gather x0 -> x1, local copies, waits for them, and re-layouts: none -> 12.2 us  [body(): lax.all_gather(expert_hidden, 'tp')]
  transfers between devices with their start and end apart: 5 -> 5, of which waited for: 4 -> 4; matrix products, arithmetic and copies ran while one was open for 4% -> 3% of each run, Pallas kernels for 0% -> 0%
where the time goes in v1:
time: 290 us; the launch traced here: 289 us
  waiting for transfers between devices  146 us (50%)
  blocking collectives  42.4 us (15%)
  local copies, waits for them, and re-layouts  36.9 us (13%)
  matrix products  30.9 us (11%)
  between operations  13.3 us (5%)
  starting transfers between devices  10.6 us (4%)
  other arithmetic  7.79 us (3%)
    all_gather x1, waiting for transfers between devices, body(): lax.all_gather(expert_hidden, 'tp')  58.4 us
    psum x1, waiting for transfers between devices, body(): projected = lax.psum(partial_proj, 'tp')  36 us
    all_gather x1, waiting for transfers between devices, body(): arrived = lax.all_gather(landed, 'tp', axis=2, tiled=True)  33.3 us
    all_to_all x1, blocking collectives, body(): lax.all_to_all(jnp.where((own_owners > 0)[..., None], taken, jnp.zeros(()...  30.6 us
    all_to_all x1, waiting for transfers between devices, body(): lax.all_to_all(expert_out, 'sp', split_axis=0, concat_axis=0, tiled=True)  18 us
    another operation x2, local copies, waits for them, and re-layouts  14.4 us
    all_gather x1, local copies, waits for them, and re-layouts, body(): lax.all_gather(expert_hidden, 'tp')  12.2 us
    dot_general x1, matrix products, body(): jnp.einsum('sxcf,xfd->sxcd', jnp.concatenate(lax.all_gather(expert_hidden...  10.1 us
  transfers between devices with their start and end apart: 5, of which 4 were waited for; matrix products, arithmetic and copies ran while one was open for 3% of the time, Pallas kernels for 0%

profile of v1, /device:TPU:0, one launch (start us, length us, event | category | flops | bytes accessed | tf_op | source)
XLA Modules:
  0.0 288.6 jit_solution(15837828662458275867)
XLA Ops:
  6.5 1.0 multiply_convert_fusion.1
  7.6 4.9 %collective-permute-start = (bf16[30,256]{1,0:T(8,128)(2,1)S(1)}, bf16[30,256]{1,0:T(8,128)(2,1)S(1)}, u32[]{:S(2)}, u32[]{:S(2)}) collective-permute-start(bf16[30,256]{1,0:T(8,128)(2,1)S(1)} %slice.16), channel_id=1, source_target_pairs={{0,4},{4,8},{8,12},{12,16},{16,20},{20,24},{24,28},{1,5},{5,9},{9,... | collective-permute-start | bytes 46088 | tf_op jit(solution)/shard_map/ppermute | solution.py:13
  12.5 0.7 broadcast_multiply_fusion
  13.2 0.8 copy.26
  13.9 0.1 eq.29
  14.1 0.1 eq.25
  14.2 0.1 copy.25
  14.3 0.1 mul.137
  14.4 1.1 reduce-window.6
  15.6 0.2 slice_reduce_fusion
  15.8 0.1 fusion.40
  15.9 0.7 convert_element_type.69
  16.7 2.4 scatter_custom_fusion
  19.1 0.7 broadcast_in_dim.14
  19.8 2.4 while.13
  22.3 0.1 fusion.46
  22.4 6.3 %all-reduce = (f32[128]{0:T(128)S(1)}, f32[128]{0:T(128)S(1)}) all-reduce(f32[128]{0:T(128)S(1)} %get-tuple-element.86, f32[128]{0:T(128)S(1)} %get-tuple-element.85), channel_id=1, replica_groups=mesh['sp'=8,'tp'=4] {'tp'}, use_global_device_ids=true, to_apply=%region_5.0 | all-reduce | flops 256 | bytes 2048 | tf_op jit(solution)/shard_map/psum | solution.py:57
  28.7 2.1 fusion.33
  30.9 0.0 all-gather.4.cloned.1.call-start
  30.9 0.1 add_select_fusion
  31.0 0.1 reshape.149
  31.1 0.1 compare_bitcast_fusion
  31.2 36.0 %all-reduce.3.cloned.1.call-done = f32[128,2048]{1,0:T(8,128)} async-done(((f32[128,2048]{1,0:T(8,128)}), f32[128,2048]{1,0:T(8,128)}) %all-reduce.3.cloned.1.call-update) | async-done | bytes 1048592 | tf_op jit(solution)/shard_map/psum | solution.py:65
  67.2 1.5 fusion.30
  68.7 0.2 fusion.32
  68.9 1.4 gather_fusion
  70.2 0.1 broadcast_select_fusion
  70.4 30.6 %all_to_all.10 = bf16[8,1,32,2048]{3,2,1,0:T(8,128)(2,1)} all-to-all(bf16[8,1,32,2048]{3,2,1,0:T(8,128)(2,1)S(1)} %broadcast_select_fusion), channel_id=1, replica_groups=mesh['sp'=8,'tp'=4] {'sp'}, dimensions={0} | all-to-all | bytes 2097152 | tf_op jit(solution)/shard_map/all_to_all | solution.py:102
  101.0 0.0 all-gather.4.cloned.1.call-update
  101.0 0.2 all-gather.6.cloned.1.call-start
  101.3 33.3 %all-gather.4.cloned.1.call-done = bf16[8,1,128,2048]{3,2,0,1:T(8,128)(2,1)} async-done(((bf16[8,1,32,2048]{3,2,0,1:T(8,128)(2,1)}), bf16[8,1,128,2048]{3,2,0,1:T(8,128)(2,1)}) %all-gather.4.cloned.1.call-update) | async-done | bytes 4194320 | tf_op jit(solution)/shard_map/all_gather | solution.py:109
  134.5 7.6 %fusion.3 = f32[8,128,1024]{2,1,0:T(8,128)S(1)} fusion(bf16[1,2048,1024]{2,1,0:T(8,128)(2,1)} %param.31, bf16[8,1,128,2048]{3,2,0,1:T(8,128)(2,1)} %all-gather.4.cloned.1.call-done), kind=kOutput, calls=%fused_computation.10 | convolution fusion | flops 4294967296 | bytes 12582912 | tf_op jit(solution)/shard_map/sxcd,xdf->sxcf/dot_general | solution.py:111
  142.2 6.4 %fusion.16 = bf16[8,1,128,1024]{3,2,1,0:T(8,128)(2,1)} fusion(f32[8,128,1024]{2,1,0:T(8,128)S(1)} %fusion.3, bf16[1,2048,1024]{2,1,0:T(8,128)(2,1)S(1)} %copy-done.4, bf16[8,1,128,2048]{3,2,0,1:T(8,128)(2,1)S(1)} %copy-done.5), kind=kOutput, calls=%fused_computation.21 | convolution fusion | flops 4301258752 | bytes 14680064 | tf_op jit(solution)/shard_map/sxcd,xdf->sxcf/dot_general | solution.py:110
  148.6 0.0 all-gather.6.cloned.1.call-update
  148.6 58.4 %all-gather.6.cloned.1.call-done = bf16[32,1,128,1024]{3,2,1,0:T(8,128)(2,1)} async-done(((bf16[8,1,128,1024]{3,2,1,0:T(8,128)(2,1)}), bf16[32,1,128,1024]{3,2,1,0:T(8,128)(2,1)}) %all-gather.6.cloned.1.call-update) | async-done | bytes 8388624 | tf_op jit(solution)/shard_map/all_gather | solution.py:116
  207.0 12.2 %copy.35 = bf16[4,8,1,128,1024]{4,0,3,1,2:T(4,128)(2,1)} copy(bf16[4,8,1,128,1024]{4,3,1,0,2:T(8,128)(2,1)} %bitcast.109) | data formatting | bytes 16777216 | tf_op jit(solution)/shard_map/all_gather | solution.py:116
  219.2 14.4 %reshape.155 = bf16[8,128,4096]{2,1,0:T(8,128)(2,1)} reshape(bf16[8,1,128,4,1024]{4,3,2,0,1:T(4,128)(2,1)} %bitcast.107) | data formatting | bytes 16777216 | tf_op jit(solution)/shard_map/reshape.19
  233.5 10.1 %fusion.24 = bf16[8,1,128,512]{3,2,1,0:T(8,128)(2,1)} fusion(bf16[8,128,4096]{2,1,0:T(8,128)(2,1)} %reshape.155, bf16[1,4096,512]{2,1,0:T(8,128)(2,1)} %param.32), kind=kOutput, calls=%fused_computation.23 | convolution fusion | flops 4295491584 | bytes 13631488 | tf_op jit(solution)/shard_map/sxcf,xfd->sxcd/dot_general | solution.py:114
  243.7 5.5 %all-to-all-start.1 = ((bf16[8,1,128,512]{3,2,1,0:T(8,128)(2,1)}), bf16[8,1,128,512]{3,2,1,0:T(8,128)(2,1)S(1)}, u32[]{:S(2)}, u32[]{:S(2)}) async-start(bf16[8,1,128,512]{3,2,1,0:T(8,128)(2,1)} %fusion.24), calls=%async_computation.1 | async-start | bytes 2097152 | tf_op jit(solution)/shard_map/all_to_all | solution.py:121
  249.2 0.1 copy.33
  249.3 1.3 fusion.47
  250.6 1.3 fusion.29
  252.0 5.4 %all_gather.12 = bf16[128,512]{1,0:T(8,128)(2,1)S(1)} all-gather(bf16[128,128]{1,0:T(8,128)(2,1)S(1)} %fusion.29), channel_id=1, replica_groups=mesh['sp'=8,'tp'=4] {'tp'}, dimensions={1}, use_global_device_ids=true | all-gather | bytes 163840 | tf_op jit(solution)/shard_map/all_gather | solution.py:76
  257.4 18.0 %all-to-all-done.1 = bf16[8,1,128,512]{3,2,1,0:T(8,128)(2,1)S(1)} async-done(((bf16[8,1,128,512]{3,2,1,0:T(8,128)(2,1)}), bf16[8,1,128,512]{3,2,1,0:T(8,128)(2,1)S(1)}, u32[]{:S(2)}, u32[]{:S(2)}) %all-to-all-start.1) | async-done | bytes 1048608 | tf_op jit(solution)/shard_map/all_to_all | solution.py:121
  275.4 2.6 gather_fusion.1
  278.0 1.4 reshape.158
  279.4 0.7 multiply_reduce_fusion
  280.1 1.9 fusion.28
  (89 shorter events, 1.7 us)
Async XLA Ops:
  6.5 22.2 %copy-start = (bf16[256,2048]{1,0:T(8,128)(2,1)S(1)}, bf16[256,2048]{1,0:T(8,128)(2,1)}, u32[]{:S(2)}) copy-start(bf16[256,2048]{1,0:T(8,128)(2,1)} %param.26) | copy-start | bytes 3145732
  6.5 60.6 %copy-start.1 = (bf16[128,2048]{1,0:T(8,128)(2,1)S(1)}, bf16[128,2048]{1,0:T(8,128)(2,1)}, u32[]{:S(2)}) copy-start(bf16[128,2048]{1,0:T(8,128)(2,1)} %param.19) | copy-start | bytes 1572868
  6.5 60.6 %all-reduce.3.cloned.1.call-start = ((), (), s32[]{:S(2)}) async-start(), calls=%async_computation.2 | async-start | bytes 2097152 | tf_op jit(solution)/shard_map/psum | solution.py:65
  7.6 11.5 %collective-permute-start = (bf16[30,256]{1,0:T(8,128)(2,1)S(1)}, bf16[30,256]{1,0:T(8,128)(2,1)S(1)}, u32[]{:S(2)}, u32[]{:S(2)}) collective-permute-start(bf16[30,256]{1,0:T(8,128)(2,1)S(1)} %slice.16), channel_id=1, source_target_pairs={{0,4},{4,8},{8,12},{12,16},{16,20},{20,24},{24,28},{1,5},{5,9},{9,... | collective-permute-start | bytes 46088 | tf_op jit(solution)/shard_map/ppermute | solution.py:13
  14.2 54.5 %copy-start.2 = (f32[2048]{0:T(1024)S(1)}, f32[2048]{0:T(1024)}, u32[]{:S(2)}) copy-start(f32[2048]{0:T(1024)} %param.27) | copy-start | bytes 24580
  30.9 103.7 %all-gather.4.cloned.1.call-start = ((), (), s32[]{:S(2)}) async-start(), calls=%async_computation.3 | async-start | bytes 5242880 | tf_op jit(solution)/shard_map/all_gather | solution.py:109
  101.0 106.0 %all-gather.6.cloned.1.call-start = ((), (), s32[]{:S(2)}) async-start(), calls=%async_computation.4 | async-start | bytes 10485760 | tf_op jit(solution)/shard_map/all_gather | solution.py:116
  134.5 7.7 %copy-start.4 = (bf16[1,2048,1024]{2,1,0:T(8,128)(2,1)S(1)}, bf16[1,2048,1024]{2,1,0:T(8,128)(2,1)}, u32[]{:S(2)}) copy-start(bf16[1,2048,1024]{2,1,0:T(8,128)(2,1)} %param.30) | copy-start | bytes 12582916
  134.5 7.7 %copy-start.5 = (bf16[8,1,128,2048]{3,2,0,1:T(8,128)(2,1)S(1)}, bf16[8,1,128,2048]{3,2,0,1:T(8,128)(2,1)}, u32[]{:S(2)}) copy-start(bf16[8,1,128,2048]{3,2,0,1:T(8,128)(2,1)} %all-gather.4.cloned.1.call-done) | copy-start | bytes 12582916
  233.5 15.7 %copy-start.3 = (f32[128,4]{0,1:T(4,128)S(1)}, f32[128,4]{0,1:T(4,128)}, u32[]{:S(2)}) copy-start(f32[128,4]{0,1:T(4,128)} %param.29) | copy-start | bytes 6148
  243.7 31.7 %all-to-all-start.1 = ((bf16[8,1,128,512]{3,2,1,0:T(8,128)(2,1)}), bf16[8,1,128,512]{3,2,1,0:T(8,128)(2,1)S(1)}, u32[]{:S(2)}, u32[]{:S(2)}) async-start(bf16[8,1,128,512]{3,2,1,0:T(8,128)(2,1)} %fusion.24), calls=%async_computation.1 | async-start | bytes 2097152 | tf_op jit(solution)/shard_map/all_to_all | solution.py:121
Sparse Core Ops, SparseCore 0:
  31.0 36.1 all-reduce.2
  101.2 33.3 all-gather.3
  148.7 58.2 all-gather.5
